TPU v7x, 256 devices: a whole 4x4x8 slice. The times are simulated.
256 devices in a mesh: gr: 2 (over z_hi), sp: 16 (over z_lo, y), tp: 8 (over x, core).
Axes of the slice: x: 4, y: 4, z: 8 (z_hi: 2, z_lo: 4; z = z_hi * 4 + z_lo), core: 2. Of those that a mesh axis runs over, the one named last changes fastest.
Arguments:
- tokens: bfloat16 [8, 3072, 4096], P('gr', 'sp', 'tp'), may hold values from -6.5 to 6.5
- first_token_input: bfloat16 [8, 4096], P('gr', 'sp'), may hold values from -6 to 6
- forget_weight: bfloat16 [4096, 4096], P(None, 'tp'), may hold values from -0.1171875 to 0.1171875
- value_weight: bfloat16 [4096, 4096], P(None, 'tp'), may hold values from -0.375 to 0.375
- query_weight: bfloat16 [4096, 4096], P('sp', 'tp'), may hold values from -0.09375 to 0.09375
- output_gate_weight: bfloat16 [4096, 4096], P('sp', 'tp'), may hold values from -0.09375 to 0.09375
- forget_bound_slack: float32 [4096], P('tp'), may hold values from 0.00016276042 to 0.8, as said below
- additional_damping_exponent: float32 [8, 3072, 32], P('gr', 'sp', 'tp'), may hold values from -2.2 to 0, as said below
- read_norm_scale: float32 [128], replicated, may hold values from 0.1 to 1.9
Outputs:
- cache: bfloat16 [8, 32, 128, 128], P('gr', 'tp', 'sp')
- first_read: bfloat16 [8, 4096], P('gr', 'tp')
Inputs may be any that keep to these rules, and one draw needn't show every extreme that they name: `forget_bound_slack`: positive gaps, one per channel. `additional_damping_exponent`: non-positive log-decays.
All inputs are finite; a program needn't handle non-finite values.
Results may differ from a plain program's by a relative error of at most 0.018.
Values may be sent and summed in bfloat16 or wider, within the bound.
No kernel may reach another device: no remote copies, remote signals or barrier semaphores. Data moves between devices by JAX's collectives and lax.ppermute only.
A program may use at most 64 MiB of HBM per device.

v0:
```python
import jax
import jax.numpy as jnp
from jax import lax
from jax.sharding import PartitionSpec as P


def from_everyone(shard, axis):
    count = lax.axis_size(axis)
    return lax.all_to_all(
        jnp.broadcast_to(shard[None], (count, *shard.shape)), axis, 0, 0, tiled=True
    )


def folded_in_pairs(pieces, combine):
    while len(jax.tree.leaves(pieces)[0]) > 1:
        pieces = jax.vmap(combine)(*(pieces[side::2] for side in (0, 1)))
    return pieces[0]


def prefix(shard, axis, combine, identity):
    count, position = (lax.axis_size(axis), lax.axis_index(axis))
    passed = jnp.arange(count) > position

    def kept(part, zero, own):
        part = jnp.where(
            passed.reshape(-1, *(1 for _ in own.shape)), part, jnp.asarray(zero, own.dtype)
        )
        return part[::-1]

    pieces = from_everyone(shard, axis)
    return folded_in_pairs(kept(pieces, identity, shard), combine)


def cut_along(shard, dim, count):
    shape = shard.shape
    blocks = shard.reshape(*shape[:dim], count, shape[dim] // count, *shape[dim + 1 :])
    return jnp.moveaxis(blocks, dim, 0)


def sent_and_summed(shard, axis, dim):
    count = lax.axis_size(axis)
    blocks = lax.all_to_all(cut_along(shard, dim, count), axis, 0, 0, tiled=True)
    return jnp.sum(blocks.astype(jnp.float32), axis=0)


def of_everyone(shard, axis):
    everything = from_everyone(shard, axis)
    return jnp.sum(everything, axis=0)


def packed_total(arrays, axis):
    ends = [0]
    for a in arrays:
        ends.append(ends[-1] + a.size)
    total = of_everyone(jnp.concatenate([a.ravel() for a in arrays]), axis)
    return tuple((total[b:e].reshape(a.shape) for a, b, e in zip(arrays, ends, ends[1:])))


def add_sums(earlier, later_part):
    return earlier + later_part


def per_device(
    tokens,
    first_token_input,
    forget_weight,
    value_weight,
    query_weight,
    output_gate_weight,
    forget_bound_slack,
    additional_damping_exponent,
    read_norm_scale,
):
    seq_count, block_len, width_part = tokens.shape
    head_dim = read_norm_scale.shape[0]
    local_heads = additional_damping_exponent.shape[2]
    channels = local_heads * head_dim
    flat_rows = tokens.reshape(seq_count * block_len, width_part)
    segment = lax.all_gather(flat_rows, "tp", axis=1, tiled=True)
    forget_acc = jnp.dot(segment, forget_weight, preferred_element_type=jnp.float32)
    value_acc = jnp.dot(segment, value_weight, preferred_element_type=jnp.float32)
    forget = forget_acc.astype(jnp.bfloat16).reshape(seq_count, block_len, channels)
    values = value_acc.astype(jnp.bfloat16).reshape(seq_count, block_len, local_heads, head_dim)
    sp_count = lax.axis_size("sp")
    rows_here = head_dim // sp_count
    row_start = lax.axis_index("sp") * rows_here
    valve_sampler_seeds = forget_bound_slack * jax.nn.sigmoid(-forget.astype(jnp.float32))
    damping_exponent = jnp.log1p(-valve_sampler_seeds) + jnp.repeat(
        additional_damping_exponent, head_dim, axis=2
    )
    totals = jnp.sum(damping_exponent, axis=1)
    later_sum = prefix(totals, "sp", add_sums, jnp.zeros_like(totals))
    within = totals[:, None, :] - jnp.cumsum(damping_exponent, axis=1)
    weighted = (valve_sampler_seeds * jnp.exp(within + later_sum[:, None, :])).astype(jnp.bfloat16)
    weighted = weighted.reshape(seq_count, block_len, local_heads, head_dim)
    state_terms = jnp.einsum(
        "slha,slhb->shab", weighted, values, preferred_element_type=jnp.float32
    )
    state_sum = sent_and_summed(state_terms.astype(jnp.bfloat16), "sp", 2)
    cache_rows = state_sum.astype(jnp.bfloat16)
    slab_rows = first_token_input.shape[1]
    row_first = lax.axis_index("sp") * slab_rows
    forget_rows = lax.dynamic_slice_in_dim(forget_weight, row_first, slab_rows, 0)
    value_rows = lax.dynamic_slice_in_dim(value_weight, row_first, slab_rows, 0)
    new_sums = packed_total(
        (
            jnp.dot(first_token_input, query_weight, preferred_element_type=jnp.float32),
            jnp.dot(first_token_input, output_gate_weight, preferred_element_type=jnp.float32),
            jnp.dot(first_token_input, forget_rows, preferred_element_type=jnp.float32),
            jnp.dot(first_token_input, value_rows, preferred_element_type=jnp.float32),
        ),
        "sp",
    )
    new_query, new_gate, new_forget, new_value = [
        summed.astype(jnp.bfloat16) for summed in new_sums
    ]
    new_keys = (forget_bound_slack * jax.nn.sigmoid(-new_forget.astype(jnp.float32))).reshape(
        seq_count, local_heads, head_dim
    )
    own_keys = lax.dynamic_slice_in_dim(new_keys, row_start, rows_here, 2)
    own_query = lax.dynamic_slice_in_dim(
        new_query.astype(jnp.float32).reshape(seq_count, local_heads, head_dim),
        row_start,
        rows_here,
        2,
    )
    value_new = new_value.astype(jnp.float32).reshape(seq_count, local_heads, head_dim)
    updated = (1.0 - own_keys)[..., None] * cache_rows.astype(jnp.float32) + own_keys[
        ..., None
    ] * value_new[:, :, None, :]
    read_part = jnp.einsum("sha,shab->shb", own_query, updated, precision=lax.Precision.HIGHEST)
    read_sum = of_everyone(read_part, "sp")
    scaled = (
        read_sum
        * lax.rsqrt(jnp.mean(read_sum * read_sum, axis=-1, keepdims=True) + 1e-06)
        * read_norm_scale
    )
    first_read = (
        scaled.reshape(seq_count, channels) * jax.nn.silu(new_gate.astype(jnp.float32))
    ).astype(jnp.bfloat16)
    return (cache_rows, first_read)


def solution(mesh):
    placed = (
        P("gr", "sp", "tp"),
        P("gr", "sp"),
        P(None, "tp"),
        P(None, "tp"),
        P("sp", "tp"),
        P("sp", "tp"),
        P("tp"),
        P("gr", "sp", "tp"),
        P(),
    )
    return jax.shard_map(
        per_device,
        mesh=mesh,
        in_specs=placed,
        out_specs=(P("gr", "tp", "sp", None), P("gr", "tp")),
        check_vma=False,
    )
```

profile of v0, /device:TPU:2, one launch (start us, length us, event | category | flops | bytes accessed | tf_op | source)
XLA Modules:
  0.0 156.7 jit_solution(15677566617659732985)
XLA Ops:
  7.2 0.7 all-gather.2.cloned.1.call-update
  8.1 0.8 convolution_bitcast_fusion.3
  8.9 1.1 convolution_bitcast_fusion.2
  10.1 1.1 convolution_bitcast_fusion.1
  11.2 1.1 convolution_bitcast_fusion
  12.5 1.0 broadcast_in_dim.20
  13.5 1.8 %reshape.149 = f32[4,192,512]{2,1,0:T(8,128)} reshape(f32[4,192,4,128]{3,2,1,0:T(4,128)S(1)} %broadcast_in_dim.20) | data formatting | bytes 3145728 | tf_op jit(solution)/shard_map/reshape | solution.py:88
  15.3 40.1 %all-gather.2.cloned.1.call-done = bf16[768,4096]{1,0:T(8,128)(2,1)} async-done(((bf16[768,512]{1,0:T(8,128)(2,1)}), bf16[768,4096]{1,0:T(8,128)(2,1)}) %all-gather.2.cloned.1.call-update) | async-done | bytes 6291472 | tf_op jit(solution)/shard_map/all_gather | solution.py:79
  55.3 7.4 %convolution_convert_fusion = bf16[768,512]{1,0:T(8,128)(2,1)S(1)} fusion(bf16[768,4096]{1,0:T(8,128)(2,1)} %all-gather.2.cloned.1.call-done, bf16[4096,512]{1,0:T(8,128)(2,1)} %param.12), kind=kOutput, calls=%fused_computation.10 | convolution fusion | flops 3221618688 | bytes 11272192 | tf_op jit(solution)/shard_map/dot_general | solution.py:81
  62.7 1.1 reshape.153
  63.9 7.0 %add_divide_fusion = f32[768,512]{1,0:T(8,128)S(1)} fusion(bf16[768,4096]{1,0:T(8,128)(2,1)} %all-gather.2.cloned.1.call-done, bf16[4096,512]{1,0:T(8,128)(2,1)} %param.11), kind=kOutput, calls=%fused_computation.9 | convolution fusion | flops 3222798336 | bytes 12058624 | tf_op jit(solution)/shard_map/dot_general | solution.py:80
  70.8 0.5 div.22
  71.5 2.4 %add_reduce_fusion = f32[4,4,128]{2,1,0:T(4,128)S(1)} fusion(f32[4,192,4,128]{3,2,1,0:T(4,128)S(1)} %div.22, f32[4,192,4]{2,1,0:T(8,128)} %copy-done.2, f32[4,128]{1,0:T(4,128)S(1)} %bitcast.77), kind=kLoop, calls=%fused_computation.8 | loop fusion | flops 1570816 | bytes 1595392 | tf_op jit(solution)/shard_map/reduce_sum | solution.py:91
  73.9 0.7 broadcast_in_dim.22
  74.6 7.4 %all-to-all-start = ((f32[16,4,512]{2,1,0:T(4,128)}), f32[16,4,512]{2,1,0:T(4,128)S(1)}, u32[]{:S(2)}, u32[]{:S(2)}) async-start(f32[16,4,512]{2,1,0:T(4,128)} %broadcast_in_dim.22), calls=%async_computation | async-start | bytes 262144 | tf_op jit(solution)/shard_map/all_to_all | solution.py:9
  82.0 2.0 %add_bitcast_fusion = f32[4,512,192]{1,2,0:T(8,128)S(1)} fusion(f32[4,192,512]{2,1,0:T(8,128)} %reshape.149, f32[4,192,512]{2,1,0:T(8,128)S(1)} %bitcast.70, f32[512]{0:T(512)S(1)} %copy-done.5), kind=kLoop, calls=%fused_computation.7 | loop fusion | flops 1179648 | bytes 4720640 | tf_op jit(solution)/shard_map/transpose
  84.3 1.6 %fusion = f32[4,512,2,128]{1,2,3,0:T(2,128)S(1)} fusion(f32[4,512,2,128]{1,3,2,0:T(8,128)S(1)} %bitcast.72), kind=kOutput, calls=%fused_computation | output fusion | flops 66584576 | bytes 4194304 | tf_op jit(solution)/shard_map/reduce-window
  85.9 1.3 copy-done.1
  87.3 2.3 %broadcast_add_fusion = f32[4,512,2,128]{1,2,3,0:T(2,128)S(1)} fusion(f32[4,512,2,128]{1,2,3,0:T(2,128)} %copy-done.1, f32[4,512,2]{1,2,0:T(2,128)S(1)} %slice.107), kind=kLoop, calls=%fused_computation.18 | loop fusion | flops 524288 | bytes 4210688 | tf_op jit(solution)/shard_map/reduce_window_sum
  89.7 1.7 %copy.32 = f32[4,512,2,128]{1,3,2,0:T(8,128)} copy(f32[4,512,2,128]{1,2,3,0:T(2,128)S(1)} %broadcast_add_fusion) | data formatting | bytes 4194304 | tf_op jit(solution)/shard_map/reduce_window_sum
  91.4 1.2 broadcast_in_dim.24
  92.6 7.5 %all-to-all-start.2 = ((f32[16,1,8192]{2,1,0:T(1,128)}), f32[16,1,8192]{2,1,0:T(1,128)S(1)}, u32[]{:S(2)}, u32[]{:S(2)}) async-start(f32[16,1,8192]{2,1,0:T(1,128)} %broadcast_in_dim.24), calls=%async_computation.2 | async-start | bytes 1048576 | tf_op jit(solution)/shard_map/all_to_all | solution.py:9
  100.3 2.1 %fusion.6 = bf16[4,4,16,8,128]{4,3,2,1,0:T(8,128)(2,1)S(1)} fusion(bf16[4,192,4,128]{3,2,1,0:T(4,128)(2,1)S(1)} %copy-done.3, f32[4,256,512]{2,1,0:T(8,128)} %bitcast.73, f32[4,192,512]{2,1,0:T(8,128)S(1)} %bitcast.71, f32[4,512]{1,0:T(4,128)S(1)} %fusion.22, f32[4,512]{1,0:T(4,128)S(1)} %bitcast.76, f32[512]{0:T(512)S(1)} %copy-done.5), kind=kOutput, calls=%fused_computation.13 | convolution fusion | flops 102891520 | bytes 4474880 | tf_op jit(solution)/shard_map/slha,slhb->shab/dot_general | solution.py:96
  102.4 0.9 copy.64
  103.3 12.0 %all-to-all-done.2 = f32[16,1,8192]{2,1,0:T(1,128)S(1)} async-done(((f32[16,1,8192]{2,1,0:T(1,128)}), f32[16,1,8192]{2,1,0:T(1,128)S(1)}, u32[]{:S(2)}, u32[]{:S(2)}) %all-to-all-start.2) | async-done | bytes 524320 | tf_op jit(solution)/shard_map/all_to_all | solution.py:9
  115.3 4.6 %all-to-all-start.1 = ((bf16[16,4,4,8,128]{4,3,2,1,0:T(8,128)(2,1)}), bf16[16,4,4,8,128]{4,3,2,1,0:T(8,128)(2,1)S(1)}, u32[]{:S(2)}, u32[]{:S(2)}) async-start(bf16[16,4,4,8,128]{4,3,2,1,0:T(8,128)(2,1)} %bitcast.68), calls=%async_computation.1 | async-start | bytes 1048576 | tf_op jit(solution)/shard_map/all_to_all | solution.py:42
  120.0 0.4 reduce_sum.50
  120.6 14.1 %all-to-all-done.1 = bf16[16,4,4,8,128]{4,3,2,1,0:T(8,128)(2,1)S(1)} async-done(((bf16[16,4,4,8,128]{4,3,2,1,0:T(8,128)(2,1)}), bf16[16,4,4,8,128]{4,3,2,1,0:T(8,128)(2,1)S(1)}, u32[]{:S(2)}, u32[]{:S(2)}) %all-to-all-start.1) | async-done | bytes 524320 | tf_op jit(solution)/shard_map/all_to_all | solution.py:42
  135.0 0.7 broadcast_in_dim.25
  135.7 4.4 %all-to-all-start.3 = ((f32[16,4,4,128]{3,2,1,0:T(4,128)}), f32[16,4,4,128]{3,2,1,0:T(4,128)S(1)}, u32[]{:S(2)}, u32[]{:S(2)}) async-start(f32[16,4,4,128]{3,2,1,0:T(4,128)} %broadcast_in_dim.25), calls=%async_computation.3 | async-start | bytes 262144 | tf_op jit(solution)/shard_map/all_to_all | solution.py:9
  140.2 8.9 %all-to-all-done.3 = f32[16,4,4,128]{3,2,1,0:T(4,128)S(1)} async-done(((f32[16,4,4,128]{3,2,1,0:T(4,128)}), f32[16,4,4,128]{3,2,1,0:T(4,128)S(1)}, u32[]{:S(2)}, u32[]{:S(2)}) %all-to-all-start.3) | async-done | bytes 131104 | tf_op jit(solution)/shard_map/all_to_all | solution.py:9
  149.3 0.6 fusion.24
  (53 shorter events, 1.9 us)
Async XLA Ops:
  7.2 1.0 copy-start
  7.2 4.0 %copy-start.4 = (bf16[4,256]{1,0:T(4,128)(2,1)S(1)}, bf16[4,256]{1,0:T(4,128)(2,1)}, u32[]{:S(2)}) copy-start(bf16[4,256]{1,0:T(4,128)(2,1)} %param.10) | copy-start | bytes 6148
  7.2 5.1 %copy-start.7 = (f32[4,192,4]{1,2,0:T(4,128)S(1)}, f32[4,192,4]{1,2,0:T(4,128)}, u32[]{:S(2)}) copy-start(f32[4,192,4]{1,2,0:T(4,128)} %param.16) | copy-start | bytes 36868
  7.2 48.1 %all-gather.2.cloned.1.call-start = ((), (), s32[]{:S(2)}) async-start(), calls=%async_computation.4 | async-start | bytes 7077888 | tf_op jit(solution)/shard_map/all_gather | solution.py:79
  12.5 2.8 %copy-start.2 = (f32[4,192,4]{2,1,0:T(8,128)}, f32[4,192,4]{2,1,0:T(8,128)S(1)}, u32[]{:S(2)}) copy-start(f32[4,192,4]{2,1,0:T(8,128)S(1)} %copy.30) | copy-start | bytes 36868
  70.8 0.7 copy-start.5
  74.6 16.8 %all-to-all-start = ((f32[16,4,512]{2,1,0:T(4,128)}), f32[16,4,512]{2,1,0:T(4,128)S(1)}, u32[]{:S(2)}, u32[]{:S(2)}) async-start(f32[16,4,512]{2,1,0:T(4,128)} %broadcast_in_dim.22), calls=%async_computation | async-start | bytes 262144 | tf_op jit(solution)/shard_map/all_to_all | solution.py:9
  85.9 1.3 copy-start.1
  91.4 8.9 %copy-start.3 = (bf16[4,192,4,128]{3,2,1,0:T(4,128)(2,1)S(1)}, bf16[4,192,4,128]{3,2,1,0:T(4,128)(2,1)}, u32[]{:S(2)}) copy-start(bf16[4,192,4,128]{3,2,1,0:T(4,128)(2,1)} %reshape.153) | copy-start | bytes 2359300
  92.6 22.8 %all-to-all-start.2 = ((f32[16,1,8192]{2,1,0:T(1,128)}), f32[16,1,8192]{2,1,0:T(1,128)S(1)}, u32[]{:S(2)}, u32[]{:S(2)}) async-start(f32[16,1,8192]{2,1,0:T(1,128)} %broadcast_in_dim.24), calls=%async_computation.2 | async-start | bytes 1048576 | tf_op jit(solution)/shard_map/all_to_all | solution.py:9
  115.3 24.8 %copy-start.8 = (f32[128]{0:T(128)S(1)}, f32[128]{0:T(128)}, u32[]{:S(2)}) copy-start(f32[128]{0:T(128)} %param.17) | copy-start | bytes 1540
  115.3 19.3 %all-to-all-start.1 = ((bf16[16,4,4,8,128]{4,3,2,1,0:T(8,128)(2,1)}), bf16[16,4,4,8,128]{4,3,2,1,0:T(8,128)(2,1)S(1)}, u32[]{:S(2)}, u32[]{:S(2)}) async-start(bf16[16,4,4,8,128]{4,3,2,1,0:T(8,128)(2,1)} %bitcast.68), calls=%async_computation.1 | async-start | bytes 1048576 | tf_op jit(solution)/shard_map/all_to_all | solution.py:42
  134.8 15.1 %copy-start.6 = (bf16[4,4,8,128]{3,2,1,0:T(8,128)(2,1)}, bf16[4,4,8,128]{3,2,1,0:T(8,128)(2,1)S(1)}, u32[]{:S(2)}) copy-start(bf16[4,4,8,128]{3,2,1,0:T(8,128)(2,1)S(1)} %reduce_sum.49) | copy-start | bytes 98308
  135.7 13.4 %all-to-all-start.3 = ((f32[16,4,4,128]{3,2,1,0:T(4,128)}), f32[16,4,4,128]{3,2,1,0:T(4,128)S(1)}, u32[]{:S(2)}, u32[]{:S(2)}) async-start(f32[16,4,4,128]{3,2,1,0:T(4,128)} %broadcast_in_dim.25), calls=%async_computation.3 | async-start | bytes 262144 | tf_op jit(solution)/shard_map/all_to_all | solution.py:9
Sparse Core Ops, SparseCore 0:
  9.8 45.4 all-gather.1
where the time goes:
time: 157 us
  waiting for transfers between devices  75.7 us (48%)
  starting transfers between devices  24 us (15%)
  matrix products  20.8 us (13%)
  between operations  14.3 us (9%)
  local copies, waits for them, and re-layouts  11.9 us (8%)
  other arithmetic  10 us (6%)
    all_gather x1, waiting for transfers between devices, per_device(): segment = lax.all_gather(flat_rows, 'tp', axis=1, tiled=True)  40.1 us
    all_to_all x3, waiting for transfers between devices, from_everyone(): lax.all_to_all(jnp.broadcast_to(shard[None], (count, *shard.shape)), axis...  20.9 us
    all_to_all x3, starting transfers between devices, from_everyone(): lax.all_to_all(jnp.broadcast_to(shard[None], (count, *shard.shape)), axis...  19.3 us
    all_to_all x1, waiting for transfers between devices, sent_and_summed(): lax.all_to_all(cut_along(shard, dim, count), axis, 0, 0, tiled=True)  14.1 us
    dot_general x1, matrix products, per_device(): jnp.dot(segment, value_weight, preferred_element_type=jnp.float32)  7.4 us
    dot_general x1, matrix products, per_device(): jnp.dot(segment, forget_weight, preferred_element_type=jnp.float32)  6.97 us
    all_to_all x1, starting transfers between devices, sent_and_summed(): lax.all_to_all(cut_along(shard, dim, count), axis, 0, 0, tiled=True)  4.63 us
    another operation x3, other arithmetic  4.02 us
  transfers between devices with their start and end apart: 5, of which 4 were waited for; matrix products, arithmetic and copies ran while one was open for 12% of the time, Pallas kernels for 0%

commit v1 on v0

--- a/solution.py
+++ b/solution.py
@@ -76,7 +76,25 @@
     local_heads = additional_damping_exponent.shape[2]
     channels = local_heads * head_dim
     flat_rows = tokens.reshape(seq_count * block_len, width_part)
-    segment = lax.all_gather(flat_rows, "tp", axis=1, tiled=True)
+    size, index, rows = (lax.axis_size("tp"), lax.axis_index("tp"), flat_rows.shape[1])
+    right = [(i, (i + 1) % size) for i in range(size)]
+    left = [(i, (i - 1) % size) for i in range(size)]
+    segment = jnp.zeros(
+        (*flat_rows.shape[:1], size * rows, *flat_rows.shape[1 + 1 :]), flat_rows.dtype
+    )
+    segment = lax.dynamic_update_slice_in_dim(segment, flat_rows, index * rows, axis=1)
+    from_left = from_right = flat_rows
+    half = size // 2
+    for step in range(1, half + 1):
+        from_left = lax.ppermute(from_left, "tp", right)
+        segment = lax.dynamic_update_slice_in_dim(
+            segment, from_left, (index - step) % size * rows, axis=1
+        )
+        if step < size - half:
+            from_right = lax.ppermute(from_right, "tp", left)
+            segment = lax.dynamic_update_slice_in_dim(
+                segment, from_right, (index + step) % size * rows, axis=1
+            )
     forget_acc = jnp.dot(segment, forget_weight, preferred_element_type=jnp.float32)
     value_acc = jnp.dot(segment, value_weight, preferred_element_type=jnp.float32)
     forget = forget_acc.astype(jnp.bfloat16).reshape(seq_count, block_len, channels)

time: 157 us -> 139 us (0.89)
  the two profiles are of different devices: /device:TPU:2 before, /device:TPU:6 now
where the time goes in v1:
time: 139 us; the launch traced here: 138 us
  waiting for transfers between devices  63.7 us (46%)
  starting transfers between devices  32.9 us (24%)
  local copies, waits for them, and re-layouts  17.3 us (12%)
  matrix products  12.8 us (9%)
  other arithmetic  10.6 us (8%)
    ppermute x4, waiting for transfers between devices, per_device(): from_left = lax.ppermute(from_left, 'tp', right)  26.6 us
    all_to_all x3, waiting for transfers between devices, from_everyone(): lax.all_to_all(jnp.broadcast_to(shard[None], (count, *shard.shape)), axis...  22.1 us
    all_to_all x3, starting transfers between devices, from_everyone(): lax.all_to_all(jnp.broadcast_to(shard[None], (count, *shard.shape)), axis...  20.6 us
    all_to_all x1, waiting for transfers between devices, sent_and_summed(): lax.all_to_all(cut_along(shard, dim, count), axis, 0, 0, tiled=True)  15 us
    all_to_all x1, starting transfers between devices, sent_and_summed(): lax.all_to_all(cut_along(shard, dim, count), axis, 0, 0, tiled=True)  4.52 us
    ppermute x3, starting transfers between devices, per_device(): from_right = lax.ppermute(from_right, 'tp', left)  4.4 us
    dot_general x1, matrix products, per_device(): jnp.dot(segment, value_weight, preferred_element_type=jnp.float32)  4.34 us
    another operation x3, other arithmetic  4.01 us
  transfers between devices with their start and end apart: 11, of which 7 were waited for; matrix products, arithmetic and copies ran while one was open for 17% of the time, Pallas kernels for 0%

profile of v1, /device:TPU:6, one launch (start us, length us, event | category | flops | bytes accessed | tf_op | source)
XLA Modules:
  0.0 138.4 jit_solution(15363405005871037140)
XLA Ops:
  0.7 1.7 %collective-permute-start.1 = (bf16[768,512]{1,0:T(8,128)(2,1)}, bf16[768,512]{1,0:T(8,128)(2,1)}, u32[]{:S(2)}, u32[]{:S(2)}) collective-permute-start(bf16[768,512]{1,0:T(8,128)(2,1)} %bitcast.75), channel_id=1, source_target_pairs={{0,7},{1,0},{2,1},{3,2},{4,3},{5,4},{6,5},{7,6},{8,15},{9,8},{10,9... | collective-permute-start | bytes 2359304 | tf_op jit(solution)/shard_map/ppermute | solution.py:94
  2.4 9.9 %collective-permute-done = bf16[768,512]{1,0:T(8,128)(2,1)S(1)} collective-permute-done((bf16[768,512]{1,0:T(8,128)(2,1)}, bf16[768,512]{1,0:T(8,128)(2,1)S(1)}, u32[]{:S(2)}, u32[]{:S(2)}) %collective-permute-start) | collective-permute-done | bytes 786464 | tf_op jit(solution)/shard_map/ppermute | solution.py:89
  12.3 1.8 %collective-permute-start.3 = (bf16[768,512]{1,0:T(8,128)(2,1)}, bf16[768,512]{1,0:T(8,128)(2,1)}, u32[]{:S(2)}, u32[]{:S(2)}) collective-permute-start(bf16[768,512]{1,0:T(8,128)(2,1)} %collective-permute-done.1), channel_id=1, source_target_pairs={{0,7},{1,0},{2,1},{3,2},{4,3},{5,4},{6,5},{7,6},{8,15},{9,8},{10,9... | collective-permute-start | bytes 2359304 | tf_op jit(solution)/shard_map/ppermute | solution.py:94
  15.1 1.0 broadcast_in_dim.23
  16.0 1.8 %reshape.149 = f32[4,192,512]{2,1,0:T(8,128)} reshape(f32[4,192,4,128]{3,2,1,0:T(4,128)S(1)} %broadcast_in_dim.23) | data formatting | bytes 3145728 | tf_op jit(solution)/shard_map/reshape | solution.py:106
  17.8 6.0 %collective-permute-done.2 = bf16[768,512]{1,0:T(8,128)(2,1)} collective-permute-done((bf16[768,512]{1,0:T(8,128)(2,1)S(1)}, bf16[768,512]{1,0:T(8,128)(2,1)}, u32[]{:S(2)}, u32[]{:S(2)}) %collective-permute-start.2) | collective-permute-done | bytes 786464 | tf_op jit(solution)/shard_map/ppermute | solution.py:89
  24.7 1.1 convolution_bitcast_fusion.1
  25.8 1.1 convolution_bitcast_fusion
  29.6 5.8 %collective-permute-done.4 = bf16[768,512]{1,0:T(8,128)(2,1)S(1)} collective-permute-done((bf16[768,512]{1,0:T(8,128)(2,1)}, bf16[768,512]{1,0:T(8,128)(2,1)S(1)}, u32[]{:S(2)}, u32[]{:S(2)}) %collective-permute-start.4) | collective-permute-done | bytes 786464 | tf_op jit(solution)/shard_map/ppermute | solution.py:89
  35.4 2.3 %collective-permute-start.6 = (bf16[768,512]{1,0:T(8,128)(2,1)S(1)}, bf16[768,512]{1,0:T(8,128)(2,1)S(1)}, u32[]{:S(2)}, u32[]{:S(2)}) collective-permute-start(bf16[768,512]{1,0:T(8,128)(2,1)S(1)} %collective-permute-done.4), channel_id=1, source_target_pairs={{0,1},{1,2},{2,3},{3,4},{4,5},{5,6},{6,7},{7,0},{8,9},{9,10},{10,1... | collective-permute-start | bytes 2359304 | tf_op jit(solution)/shard_map/ppermute | solution.py:89
  37.9 1.2 constant_dynamic-update-slice_fusion.5
  39.1 1.2 constant_dynamic-update-slice_fusion.4
  40.4 1.2 constant_dynamic-update-slice_fusion.3
  41.9 4.9 %collective-permute-done.6 = bf16[768,512]{1,0:T(8,128)(2,1)S(1)} collective-permute-done((bf16[768,512]{1,0:T(8,128)(2,1)S(1)}, bf16[768,512]{1,0:T(8,128)(2,1)S(1)}, u32[]{:S(2)}, u32[]{:S(2)}) %collective-permute-start.6) | collective-permute-done | bytes 786464 | tf_op jit(solution)/shard_map/ppermute | solution.py:89
  47.0 3.6 %add_divide_fusion = f32[768,512]{1,0:T(8,128)S(1)} fusion(bf16[768,4096]{1,0:T(8,128)(2,1)S(1)} %constant_dynamic-update-slice_fusion, bf16[4096,512]{1,0:T(8,128)(2,1)S(1)} %copy-done.9), kind=kOutput, calls=%fused_computation.9 | convolution fusion | flops 3222798336 | bytes 12058624 | tf_op jit(solution)/shard_map/dot_general | solution.py:98
  50.6 4.3 %convolution_convert_fusion = bf16[768,512]{1,0:T(8,128)(2,1)} fusion(bf16[768,4096]{1,0:T(8,128)(2,1)S(1)} %constant_dynamic-update-slice_fusion, bf16[4096,512]{1,0:T(8,128)(2,1)S(1)} %copy-done.10), kind=kOutput, calls=%fused_computation.10 | convolution fusion | flops 3221618688 | bytes 11272192 | tf_op jit(solution)/shard_map/dot_general | solution.py:99
  55.6 2.4 %add_reduce_fusion = f32[4,4,128]{2,1,0:T(4,128)S(1)} fusion(f32[4,192,4,128]{3,2,1,0:T(4,128)S(1)} %div.22, f32[4,192,4]{2,1,0:T(8,128)} %copy-done.2, f32[4,128]{1,0:T(4,128)S(1)} %bitcast.79), kind=kLoop, calls=%fused_computation.8 | loop fusion | flops 1570816 | bytes 1595392 | tf_op jit(solution)/shard_map/reduce_sum | solution.py:109
  58.7 8.6 %all-to-all-start = ((f32[16,4,512]{2,1,0:T(4,128)}), f32[16,4,512]{2,1,0:T(4,128)S(1)}, u32[]{:S(2)}, u32[]{:S(2)}) async-start(f32[16,4,512]{2,1,0:T(4,128)} %broadcast_in_dim.25), calls=%async_computation | async-start | bytes 262144 | tf_op jit(solution)/shard_map/all_to_all | solution.py:9
  67.4 2.0 %add_bitcast_fusion = f32[4,512,192]{1,2,0:T(8,128)S(1)} fusion(f32[4,192,512]{2,1,0:T(8,128)} %reshape.149, f32[4,192,512]{2,1,0:T(8,128)S(1)} %bitcast.70, f32[512]{0:T(512)S(1)} %copy-done.7), kind=kLoop, calls=%fused_computation.7 | loop fusion | flops 1179648 | bytes 4720640 | tf_op jit(solution)/shard_map/transpose
  69.7 1.6 %fusion = f32[4,512,2,128]{1,2,3,0:T(2,128)S(1)} fusion(f32[4,512,2,128]{1,3,2,0:T(8,128)S(1)} %bitcast.72), kind=kOutput, calls=%fused_computation | output fusion | flops 66584576 | bytes 4194304 | tf_op jit(solution)/shard_map/reduce-window
  71.3 1.3 copy-done.1
  72.7 2.3 %broadcast_add_fusion = f32[4,512,2,128]{1,2,3,0:T(2,128)S(1)} fusion(f32[4,512,2,128]{1,2,3,0:T(2,128)} %copy-done.1, f32[4,512,2]{1,2,0:T(2,128)S(1)} %slice.107), kind=kLoop, calls=%fused_computation.18 | loop fusion | flops 524288 | bytes 4210688 | tf_op jit(solution)/shard_map/reduce_window_sum
  75.1 1.7 %copy.32 = f32[4,512,2,128]{1,3,2,0:T(8,128)} copy(f32[4,512,2,128]{1,2,3,0:T(2,128)S(1)} %broadcast_add_fusion) | data formatting | bytes 4194304 | tf_op jit(solution)/shard_map/reduce_window_sum
  77.0 2.0 %broadcast_in_dim.27 = f32[16,1,8192]{2,1,0:T(1,128)} broadcast(f32[8192]{0:T(1024)} %pad_maximum_fusion), dimensions={2} | broadcast | bytes 557056 | tf_op jit(solution)/shard_map/broadcast_in_dim | solution.py:10
  79.0 7.5 %all-to-all-start.2 = ((f32[16,1,8192]{2,1,0:T(1,128)}), f32[16,1,8192]{2,1,0:T(1,128)S(1)}, u32[]{:S(2)}, u32[]{:S(2)}) async-start(f32[16,1,8192]{2,1,0:T(1,128)} %broadcast_in_dim.27), calls=%async_computation.2 | async-start | bytes 1048576 | tf_op jit(solution)/shard_map/all_to_all | solution.py:9
  86.7 2.1 %fusion.6 = bf16[4,4,16,8,128]{4,3,2,1,0:T(8,128)(2,1)S(1)} fusion(bf16[4,192,4,128]{3,2,1,0:T(4,128)(2,1)S(1)} %reshape.153, f32[4,256,512]{2,1,0:T(8,128)} %bitcast.73, f32[4,192,512]{2,1,0:T(8,128)S(1)} %bitcast.71, f32[4,512]{1,0:T(4,128)S(1)} %fusion.22, f32[4,512]{1,0:T(4,128)S(1)} %bitcast.78, f32[512]{0:T(512)S(1)} %copy-done.7), kind=kOutput, calls=%fused_computation.13 | convolution fusion | flops 102891520 | bytes 4474880 | tf_op jit(solution)/shard_map/slha,slhb->shab/dot_general | solution.py:114
  88.8 0.9 copy.64
  89.7 13.3 %all-to-all-done.2 = f32[16,1,8192]{2,1,0:T(1,128)S(1)} async-done(((f32[16,1,8192]{2,1,0:T(1,128)}), f32[16,1,8192]{2,1,0:T(1,128)S(1)}, u32[]{:S(2)}, u32[]{:S(2)}) %all-to-all-start.2) | async-done | bytes 524320 | tf_op jit(solution)/shard_map/all_to_all | solution.py:9
  103.0 4.5 %all-to-all-start.1 = ((bf16[16,4,4,8,128]{4,3,2,1,0:T(8,128)(2,1)}), bf16[16,4,4,8,128]{4,3,2,1,0:T(8,128)(2,1)S(1)}, u32[]{:S(2)}, u32[]{:S(2)}) async-start(bf16[16,4,4,8,128]{4,3,2,1,0:T(8,128)(2,1)} %bitcast.68), calls=%async_computation.1 | async-start | bytes 1048576 | tf_op jit(solution)/shard_map/all_to_all | solution.py:42
  108.1 15.0 %all-to-all-done.1 = bf16[16,4,4,8,128]{4,3,2,1,0:T(8,128)(2,1)S(1)} async-done(((bf16[16,4,4,8,128]{4,3,2,1,0:T(8,128)(2,1)}), bf16[16,4,4,8,128]{4,3,2,1,0:T(8,128)(2,1)S(1)}, u32[]{:S(2)}, u32[]{:S(2)}) %all-to-all-start.1) | async-done | bytes 524320 | tf_op jit(solution)/shard_map/all_to_all | solution.py:42
  124.1 4.5 %all-to-all-start.3 = ((f32[16,4,4,128]{3,2,1,0:T(4,128)}), f32[16,4,4,128]{3,2,1,0:T(4,128)S(1)}, u32[]{:S(2)}, u32[]{:S(2)}) async-start(f32[16,4,4,128]{3,2,1,0:T(4,128)} %broadcast_in_dim.28), calls=%async_computation.3 | async-start | bytes 262144 | tf_op jit(solution)/shard_map/all_to_all | solution.py:9
  128.6 8.9 %all-to-all-done.3 = f32[16,4,4,128]{3,2,1,0:T(4,128)S(1)} async-done(((f32[16,4,4,128]{3,2,1,0:T(4,128)}), f32[16,4,4,128]{3,2,1,0:T(4,128)S(1)}, u32[]{:S(2)}, u32[]{:S(2)}) %all-to-all-start.3) | async-done | bytes 131104 | tf_op jit(solution)/shard_map/all_to_all | solution.py:9
  (79 shorter events, 9.4 us)
Async XLA Ops:
  0.6 26.3 %copy-start = (bf16[256,512]{1,0:T(8,128)(2,1)S(1)}, bf16[256,512]{1,0:T(8,128)(2,1)}, u32[]{:S(2)}) copy-start(bf16[256,512]{1,0:T(8,128)(2,1)} %param.13) | copy-start | bytes 786436
  0.6 11.6 %collective-permute-start = (bf16[768,512]{1,0:T(8,128)(2,1)}, bf16[768,512]{1,0:T(8,128)(2,1)S(1)}, u32[]{:S(2)}, u32[]{:S(2)}) collective-permute-start(bf16[768,512]{1,0:T(8,128)(2,1)} %bitcast.74), channel_id=1, source_target_pairs={{0,1},{1,2},{2,3},{3,4},{4,5},{5,6},{6,7},{7,0},{8,9},{9,10},{10,1... | collective-permute-start | bytes 2359304 | tf_op jit(solution)/shard_map/ppermute | solution.py:89
  0.7 11.6 %collective-permute-start.1 = (bf16[768,512]{1,0:T(8,128)(2,1)}, bf16[768,512]{1,0:T(8,128)(2,1)}, u32[]{:S(2)}, u32[]{:S(2)}) collective-permute-start(bf16[768,512]{1,0:T(8,128)(2,1)} %bitcast.75), channel_id=1, source_target_pairs={{0,7},{1,0},{2,1},{3,2},{4,3},{5,4},{6,5},{7,6},{8,15},{9,8},{10,9... | collective-permute-start | bytes 2359304 | tf_op jit(solution)/shard_map/ppermute | solution.py:94
  12.3 11.5 %collective-permute-start.2 = (bf16[768,512]{1,0:T(8,128)(2,1)S(1)}, bf16[768,512]{1,0:T(8,128)(2,1)}, u32[]{:S(2)}, u32[]{:S(2)}) collective-permute-start(bf16[768,512]{1,0:T(8,128)(2,1)S(1)} %collective-permute-done), channel_id=1, source_target_pairs={{0,1},{1,2},{2,3},{3,4},{4,5},{5,6},{6,7},{7,0},{8,9},{9,10},{10,1... | collective-permute-start | bytes 2359304 | tf_op jit(solution)/shard_map/ppermute | solution.py:89
  12.3 15.6 %collective-permute-start.3 = (bf16[768,512]{1,0:T(8,128)(2,1)}, bf16[768,512]{1,0:T(8,128)(2,1)}, u32[]{:S(2)}, u32[]{:S(2)}) collective-permute-start(bf16[768,512]{1,0:T(8,128)(2,1)} %collective-permute-done.1), channel_id=1, source_target_pairs={{0,7},{1,0},{2,1},{3,2},{4,3},{5,4},{6,5},{7,6},{8,15},{9,8},{10,9... | collective-permute-start | bytes 2359304 | tf_op jit(solution)/shard_map/ppermute | solution.py:94
  15.0 2.8 %copy-start.2 = (f32[4,192,4]{2,1,0:T(8,128)}, f32[4,192,4]{2,1,0:T(8,128)S(1)}, u32[]{:S(2)}) copy-start(f32[4,192,4]{2,1,0:T(8,128)S(1)} %copy.30) | copy-start | bytes 36868
  15.0 9.7 %copy-start.6 = (bf16[4,256]{1,0:T(4,128)(2,1)S(1)}, bf16[4,256]{1,0:T(4,128)(2,1)}, u32[]{:S(2)}) copy-start(bf16[4,256]{1,0:T(4,128)(2,1)} %param.10) | copy-start | bytes 6148
  16.0 11.1 %copy-start.5 = (bf16[256,512]{1,0:T(8,128)(2,1)S(1)}, bf16[256,512]{1,0:T(8,128)(2,1)}, u32[]{:S(2)}) copy-start(bf16[256,512]{1,0:T(8,128)(2,1)} %param.14) | copy-start | bytes 786436
  23.8 11.6 %collective-permute-start.4 = (bf16[768,512]{1,0:T(8,128)(2,1)}, bf16[768,512]{1,0:T(8,128)(2,1)S(1)}, u32[]{:S(2)}, u32[]{:S(2)}) collective-permute-start(bf16[768,512]{1,0:T(8,128)(2,1)} %collective-permute-done.2), channel_id=1, source_target_pairs={{0,1},{1,2},{2,3},{3,4},{4,5},{5,6},{6,7},{7,0},{8,9},{9,10},{10,1... | collective-permute-start | bytes 2359304 | tf_op jit(solution)/shard_map/ppermute | solution.py:89
  27.9 1.6 %copy-start.3 = (bf16[4,192,512]{2,1,0:T(8,128)(2,1)S(1)}, bf16[4,192,512]{2,1,0:T(8,128)(2,1)}, u32[]{:S(2)}) copy-start(bf16[4,192,512]{2,1,0:T(8,128)(2,1)} %param.9) | copy-start | bytes 2359300
  27.9 13.9 %collective-permute-start.5 = (bf16[768,512]{1,0:T(8,128)(2,1)}, bf16[768,512]{1,0:T(8,128)(2,1)S(1)}, u32[]{:S(2)}, u32[]{:S(2)}) collective-permute-start(bf16[768,512]{1,0:T(8,128)(2,1)} %collective-permute-done.3), channel_id=1, source_target_pairs={{0,7},{1,0},{2,1},{3,2},{4,3},{5,4},{6,5},{7,6},{8,15},{9,8},{10,9... | collective-permute-start | bytes 2359304 | tf_op jit(solution)/shard_map/ppermute | solution.py:94
  35.4 11.4 %collective-permute-start.6 = (bf16[768,512]{1,0:T(8,128)(2,1)S(1)}, bf16[768,512]{1,0:T(8,128)(2,1)S(1)}, u32[]{:S(2)}, u32[]{:S(2)}) collective-permute-start(bf16[768,512]{1,0:T(8,128)(2,1)S(1)} %collective-permute-done.4), channel_id=1, source_target_pairs={{0,1},{1,2},{2,3},{3,4},{4,5},{5,6},{6,7},{7,0},{8,9},{9,10},{10,1... | collective-permute-start | bytes 2359304 | tf_op jit(solution)/shard_map/ppermute | solution.py:89
  41.6 5.3 %copy-start.9 = (bf16[4096,512]{1,0:T(8,128)(2,1)S(1)}, bf16[4096,512]{1,0:T(8,128)(2,1)}, u32[]{:S(2)}) copy-start(bf16[4096,512]{1,0:T(8,128)(2,1)} %param.11) | copy-start | bytes 12582916
  47.0 3.7 %copy-start.10 = (bf16[4096,512]{1,0:T(8,128)(2,1)S(1)}, bf16[4096,512]{1,0:T(8,128)(2,1)}, u32[]{:S(2)}) copy-start(bf16[4096,512]{1,0:T(8,128)(2,1)} %param.12) | copy-start | bytes 12582916
  55.0 0.7 copy-start.7
  58.7 18.2 %all-to-all-start = ((f32[16,4,512]{2,1,0:T(4,128)}), f32[16,4,512]{2,1,0:T(4,128)S(1)}, u32[]{:S(2)}, u32[]{:S(2)}) async-start(f32[16,4,512]{2,1,0:T(4,128)} %broadcast_in_dim.25), calls=%async_computation | async-start | bytes 262144 | tf_op jit(solution)/shard_map/all_to_all | solution.py:9
  71.3 1.3 copy-start.1
  75.1 1.7 %copy-start.4 = (bf16[768,512]{1,0:T(8,128)(2,1)S(1)}, bf16[768,512]{1,0:T(8,128)(2,1)}, u32[]{:S(2)}) copy-start(bf16[768,512]{1,0:T(8,128)(2,1)} %convolution_convert_fusion) | copy-start | bytes 2359300
  79.0 24.0 %all-to-all-start.2 = ((f32[16,1,8192]{2,1,0:T(1,128)}), f32[16,1,8192]{2,1,0:T(1,128)S(1)}, u32[]{:S(2)}, u32[]{:S(2)}) async-start(f32[16,1,8192]{2,1,0:T(1,128)} %broadcast_in_dim.27), calls=%async_computation.2 | async-start | bytes 1048576 | tf_op jit(solution)/shard_map/all_to_all | solution.py:9
  88.8 39.9 %copy-start.11 = (f32[128]{0:T(128)S(1)}, f32[128]{0:T(128)}, u32[]{:S(2)}) copy-start(f32[128]{0:T(128)} %param.17) | copy-start | bytes 1540
  103.0 20.1 %all-to-all-start.1 = ((bf16[16,4,4,8,128]{4,3,2,1,0:T(8,128)(2,1)}), bf16[16,4,4,8,128]{4,3,2,1,0:T(8,128)(2,1)S(1)}, u32[]{:S(2)}, u32[]{:S(2)}) async-start(bf16[16,4,4,8,128]{4,3,2,1,0:T(8,128)(2,1)} %bitcast.68), calls=%async_computation.1 | async-start | bytes 1048576 | tf_op jit(solution)/shard_map/all_to_all | solution.py:42
  123.2 15.2 %copy-start.8 = (bf16[4,4,8,128]{3,2,1,0:T(8,128)(2,1)}, bf16[4,4,8,128]{3,2,1,0:T(8,128)(2,1)S(1)}, u32[]{:S(2)}) copy-start(bf16[4,4,8,128]{3,2,1,0:T(8,128)(2,1)S(1)} %reduce_sum.49) | copy-start | bytes 98308
  124.1 13.4 %all-to-all-start.3 = ((f32[16,4,4,128]{3,2,1,0:T(4,128)}), f32[16,4,4,128]{3,2,1,0:T(4,128)S(1)}, u32[]{:S(2)}, u32[]{:S(2)}) async-start(f32[16,4,4,128]{3,2,1,0:T(4,128)} %broadcast_in_dim.28), calls=%async_computation.3 | async-start | bytes 262144 | tf_op jit(solution)/shard_map/all_to_all | solution.py:9
